TPU v7x, 32 devices: a whole 2x2x4 slice. The times are simulated.
32 devices in a mesh: ep: 4 (over y, x), tp: 8 (over z, core).
Axes of the slice: x: 2, y: 2, z: 4, core: 2. Of those that a mesh axis runs over, the one named last changes fastest.
Arguments:
- mix_in: bfloat16 [4096, 2048], P(('ep', 'tp')), may hold values from -6 to 6
- mix_gain: float32 [2048], replicated, may hold values from 0.1 to 1.9
- mix_w_in: bfloat16 [2048, 512], P('tp'), may hold values from -0.125 to 0.125
- pool_mat: bfloat16 [4, 128, 128], replicated, may hold values from -0.5 to 0.5
- pool_scale: float32 [512], replicated, may hold values from 0.1 to 1.9
- mix_w_out: bfloat16 [512, 2048], P(None, 'tp'), may hold values from -0.25 to 0.25
- moe_in: bfloat16 [4096, 2048], P(('ep', 'tp')), may hold values from -6 to 6
- moe_gain: float32 [2048], replicated, may hold values from 0.1 to 1.9
- routes: int32 [4096, 2], P('ep'), may hold values from 0 to 31, all different within a row; in each aligned block of 1024 rows (0 to 1023, 1024 to 2047, ...) at most 128 rows name the same one
- route_score: bfloat16 [4096, 2], P('ep'), may hold values from 0.099609375 to 1
- exp_gate: bfloat16 [32, 2048, 768], P(('ep', 'tp')), may hold values from -0.125 to 0.125
- exp_up: bfloat16 [32, 2048, 768], P(('ep', 'tp')), may hold values from -0.125 to 0.125
- exp_down: bfloat16 [32, 768, 2048], P(('ep', 'tp')), may hold values from -0.21875 to 0.21875
- shared_gate: bfloat16 [768, 2048], P('tp'), may hold values from -0.125 to 0.125
- shared_up: bfloat16 [768, 2048], P('tp'), may hold values from -0.125 to 0.125
- shared_down: bfloat16 [768, 2048], P('tp'), may hold values from -0.21875 to 0.21875
Outputs:
- mixed: bfloat16 [4096, 2048], P(('ep', 'tp'))
- moe_out: bfloat16 [4096, 2048], P(('ep', 'tp'))
Inputs may be any that keep to these rules, and one draw needn't show every extreme that they name: `routes`: each row names 2 different experts. Within the rows of one index of ep (aligned blocks of 1024 rows) no expert is named more than 128 times, a bound that some expert reaches in some blocks.
All inputs are finite; a program needn't handle non-finite values.
Results may differ from a plain program's by a relative error of at most 0.012.
Values may be sent and summed in bfloat16 or wider, within the bound.
A program may use at most 128 MiB of HBM per device.

v0:
```python
import jax
import jax.numpy as jnp
from jax import lax
from jax.sharding import PartitionSpec as P

SEQS_MIX = 1


NORM_EPS = 1e-06
ROUTED_SCALE = 2.5


def shifted(value, axis, steps):
    count = lax.axis_size(axis)
    first, last = (max(0, -steps), min(count, count - steps))
    return lax.ppermute(value, axis, [(source, source + steps) for source in range(first, last)])


def rms_rows(values, gain):
    floats = values.astype(jnp.float32)
    scaled = floats * lax.rsqrt(jnp.mean(floats * floats, axis=-1, keepdims=True) + NORM_EPS)
    return (scaled * gain).astype(jnp.bfloat16)


def expert_ffn(rows_in, w_gate, w_up, w_down):
    row_shape = rows_in.shape
    flat_rows = rows_in.reshape(-1, row_shape[-1])
    gate_act = jnp.dot(flat_rows, w_gate, preferred_element_type=jnp.float32)
    up_act = jnp.dot(flat_rows, w_up, preferred_element_type=jnp.float32)
    hidden = (jax.nn.silu(gate_act) * up_act).astype(jnp.bfloat16)
    outputs = jnp.dot(hidden, w_down, preferred_element_type=jnp.float32).astype(jnp.bfloat16)
    return outputs.reshape(row_shape)


def shared_hidden_rows(rows_in, w_gate, w_up):
    contract = (((1,), (1,)), ((), ()))
    gate_act = lax.dot_general(rows_in, w_gate, contract, preferred_element_type=jnp.float32)
    up_act = lax.dot_general(rows_in, w_up, contract, preferred_element_type=jnp.float32)
    return (jax.nn.silu(gate_act) * up_act).astype(jnp.bfloat16)


def pool_mix(projected, prior_tail, first_row, seq_len, pool_mat, pool_scale):
    tokens, channels = projected.shape
    groups = pool_mat.shape[0]
    group_ch = pool_mat.shape[1]
    reach_rows = prior_tail.shape[0]
    extended = jnp.concatenate([prior_tail, projected], axis=0).astype(jnp.float32)
    prefix = jnp.concatenate(
        [jnp.zeros((1, channels), jnp.float32), jnp.cumsum(extended, axis=0)], axis=0
    )
    position = (first_row + lax.iota(jnp.int32, tokens)) % seq_len
    pieces = []
    for group in range(groups):
        window_len = 2 ** (group + 1)
        lower = group * group_ch
        upper = lower + group_ch
        window_sum = (
            prefix[reach_rows + 1 : reach_rows + 1 + tokens, lower:upper]
            - prefix[
                reach_rows + 1 - window_len : reach_rows + 1 - window_len + tokens, lower:upper
            ]
        )
        counts = jnp.minimum(position + 1, window_len).astype(jnp.float32)
        pieces.append(window_sum / counts[:, None] - extended[reach_rows:, lower:upper])
    pooled = jnp.concatenate(pieces, axis=1).astype(jnp.bfloat16).reshape(tokens, groups, group_ch)
    grouped = jnp.einsum("tgc,gcd->tgd", pooled, pool_mat, preferred_element_type=jnp.float32)
    return (grouped.reshape(tokens, channels) * pool_scale).astype(jnp.bfloat16)


def mixer_half(mix_in, mix_gain, pool_mat, pool_scale, joint):
    normed = rms_rows(mix_in, mix_gain)
    tokens = normed.shape[0]
    projected = jnp.dot(
        normed,
        lax.all_gather(joint[0], "tp", axis=0, tiled=True),
        preferred_element_type=jnp.float32,
    ).astype(jnp.bfloat16)
    groups = pool_mat.shape[0]
    reach_rows = 2**groups - 1
    devices = lax.axis_size("ep") * lax.axis_size("tp")
    seq_len = tokens * devices // SEQS_MIX
    first_row = lax.axis_index(("ep", "tp")) * tokens
    arrived = shifted(projected[tokens - reach_rows :], ("ep", "tp"), 1)
    prior_tail = jnp.where(first_row % seq_len == 0, jnp.zeros_like(arrived), arrived)
    pool_out = pool_mix(projected, prior_tail, first_row, seq_len, pool_mat, pool_scale)
    return jnp.dot(
        pool_out,
        lax.all_gather(joint[1], "tp", axis=1, tiled=True),
        preferred_element_type=jnp.float32,
    ).astype(jnp.bfloat16)


def expert_half(rows_all, routes, route_score, exp_gate, exp_up, exp_down, shared_weights):
    block_rows, model_width = rows_all.shape
    top_count = routes.shape[1]
    ep_count = lax.axis_size("ep")
    tp_count = lax.axis_size("tp")
    column = lax.axis_index("tp")
    capacity = 2 * block_rows * top_count // (ep_count * tp_count)
    scores = route_score.astype(jnp.float32)
    weights = scores / jnp.sum(scores, axis=1, keepdims=True) * ROUTED_SCALE
    flat_expert = routes.reshape(-1)
    flat_weight = weights.reshape(-1)
    flat_token = lax.iota(jnp.int32, block_rows * top_count) // top_count
    owned_copy = flat_expert % tp_count == column
    target = flat_expert // tp_count
    onehot = (
        (target[:, None] == lax.iota(jnp.int32, ep_count)[None, :]) & owned_copy[:, None]
    ).astype(jnp.int32)
    before = jnp.sum((jnp.cumsum(onehot, axis=0) - onehot) * onehot, axis=1)
    slot_index = jnp.where(owned_copy, target * capacity + before, ep_count * capacity)
    slot_token = (
        jnp.full((ep_count * capacity,), block_rows, jnp.int32)
        .at[slot_index]
        .set(flat_token, mode="drop")
    )
    slot_weight = (
        jnp.zeros((ep_count * capacity,), jnp.float32).at[slot_index].set(flat_weight, mode="drop")
    )
    live_slot = (slot_token < block_rows).astype(jnp.bfloat16)
    outgoing = (
        jnp.take(rows_all, jnp.minimum(slot_token, block_rows - 1), axis=0) * live_slot[:, None]
    )
    outgoing = outgoing.reshape(ep_count, capacity, model_width)
    results = expert_ffn(
        lax.all_to_all(outgoing, "ep", split_axis=0, concat_axis=0, tiled=True),
        exp_gate[0],
        exp_up[0],
        exp_down[0],
    )
    returned = lax.all_to_all(results, "ep", split_axis=0, concat_axis=0, tiled=True)
    weighted = returned.reshape(-1, model_width).astype(jnp.float32) * slot_weight[:, None]
    routed = (
        jnp.zeros((block_rows, model_width), jnp.float32).at[slot_token].add(weighted, mode="drop")
    )
    routed_sum = lax.psum_scatter(
        routed.astype(jnp.bfloat16), "tp", scatter_dimension=0, tiled=True
    ).astype(jnp.float32)
    shared_hidden = shared_hidden_rows(rows_all, shared_weights[0], shared_weights[1])
    shared_out = lax.psum_scatter(
        jnp.dot(shared_hidden, shared_weights[2], preferred_element_type=jnp.float32).astype(
            jnp.bfloat16
        ),
        "tp",
        scatter_dimension=0,
        tiled=True,
    ).astype(jnp.float32)
    return (routed_sum + shared_out).astype(jnp.bfloat16)


def shards(
    mix_in,
    mix_gain,
    mix_w_in,
    pool_mat,
    pool_scale,
    mix_w_out,
    moe_in,
    moe_gain,
    routes,
    route_score,
    exp_gate,
    exp_up,
    exp_down,
    shared_gate,
    shared_up,
    shared_down,
):
    shared_weights = (shared_gate, shared_up, shared_down)
    moe_normed = rms_rows(moe_in, moe_gain)
    joint = (mix_w_in, mix_w_out, lax.all_gather(moe_normed, "tp", axis=0, tiled=True))
    mixed = mixer_half(mix_in, mix_gain, pool_mat, pool_scale, joint)
    moe_out = expert_half(joint[2], routes, route_score, exp_gate, exp_up, exp_down, shared_weights)
    return (mixed, moe_out)


def solution(mesh):
    return jax.shard_map(
        shards,
        mesh=mesh,
        in_specs=(
            P(("ep", "tp"), None),
            P(),
            P("tp", None),
            P(),
            P(),
            P(None, "tp"),
            P(("ep", "tp"), None),
            P(),
            P("ep", None),
            P("ep", None),
            P(("ep", "tp"), None, None),
            P(("ep", "tp"), None, None),
            P(("ep", "tp"), None, None),
            P("tp", None),
            P("tp", None),
            P("tp", None),
        ),
        out_specs=(P(("ep", "tp"), None), P(("ep", "tp"), None)),
        check_vma=False,
    )
```

profile of v0, /device:TPU:0, one launch (start us, length us, event | category | flops | bytes accessed | tf_op | source)
XLA Modules:
  0.0 242.5 jit_solution(14063475898345788821)
XLA Ops:
  7.2 0.0 copy-start
  7.2 0.0 all-gather.8.cloned.1.call-start
  7.2 1.4 fusion.18
  8.6 2.0 fusion.20
  10.6 0.0 all-gather.8.cloned.1.call-update
  10.7 0.0 all-gather.4.cloned.1.call-start
  10.7 0.7 all-gather.4.cloned.1.call-update
  11.4 0.0 all-gather.6.cloned.1.call-start
  11.5 0.7 all-gather.6.cloned.1.call-update
  12.2 0.0 reduce-scatter.5.cloned.1.call-start
  12.2 48.2 %all-gather.8.cloned.1.call-done = bf16[1024,2048]{1,0:T(8,128)(2,1)} async-done(((bf16[128,2048]{1,0:T(8,128)(2,1)}), bf16[1024,2048]{1,0:T(8,128)(2,1)}) %all-gather.8.cloned.1.call-update) | async-done | bytes 4194320 | tf_op jit(solution)/shard_map/all_gather | solution.py:171
  60.4 3.7 %fusion.84 = f32[1024,96]{0,1:T(8,128)S(1)} fusion(bf16[1024,2048]{1,0:T(8,128)(2,1)} %all-gather.8.cloned.1.call-done, bf16[96,2048]{1,0:T(8,128)(2,1)} %param.29), kind=kOutput, calls=%fused_computation.149 | convolution fusion | flops 402653184 | bytes 4980736 | tf_op jit(solution)/shard_map/dot_general | solution.py:37
  64.1 6.9 %convolution_convert_fusion = bf16[1024,2048]{1,0:T(8,128)(2,1)} fusion(bf16[96,2048]{1,0:T(8,128)(2,1)} %param.31, bf16[1024,2048]{1,0:T(8,128)(2,1)} %all-gather.8.cloned.1.call-done, bf16[96,2048]{1,0:T(8,128)(2,1)} %param.30, f32[1024,96]{0,1:T(8,128)S(1)} %fusion.84), kind=kOutput, calls=%fused_computation.7 | convolution fusion | flops 807993344 | bytes 9568256 | tf_op jit(solution)/shard_map/dot_general | solution.py:141
  71.0 0.0 reduce-scatter.5.cloned.1.call-update
  71.1 0.7 copy-done.5
  71.7 1.0 copy.24
  72.8 1.3 reshape.284
  74.1 1.3 reshape.283
  75.4 1.4 reshape.282
  76.8 1.2 reduce-window.16
  77.9 0.2 slice_reduce_fusion
  78.2 0.2 reduce-window.19
  78.4 0.1 add_bitcast_fusion
  78.5 0.1 compare_select_fusion
  78.6 8.0 %scatter_custom_fusion = s32[512]{0:T(512)S(1)} fusion(s32[2048]{0:T(1024)S(1)} %bitcast.94, s32[2048]{0:T(1024)S(1)} %add_select_fusion, s32[]{:T(128)} %constant.119.clone.1), kind=kCustom, calls=%fused_computation.136 | custom fusion | bytes 2052 | tf_op jit(solution)/shard_map/scatter | solution.py:115
  86.7 8.0 %gather_fusion = bf16[512,2048]{1,0:T(8,128)(2,1)} fusion(bf16[1024,2048]{1,0:T(8,128)(2,1)} %all-gather.8.cloned.1.call-done, s32[1024]{0:T(1024)S(1)} %pad_clamp_fusion), kind=kCustom, calls=%fused_computation | custom fusion | bytes 4196352 | tf_op jit(solution)/shard_map/jit(_take)/gather | solution.py:122
  94.7 1.9 select_multiply_fusion
  96.6 0.0 copy-start.7
  96.6 29.5 %all_to_all.10 = bf16[4,128,2048]{2,1,0:T(8,128)(2,1)S(1)} all-to-all(bf16[4,128,2048]{2,1,0:T(8,128)(2,1)S(1)} %select_multiply_fusion), channel_id=1, replica_groups=mesh['ep'=4,'tp'=8] {'ep'}, dimensions={0} | all-to-all | bytes 4194304 | tf_op jit(solution)/shard_map/all_to_all | solution.py:126
  126.1 1.3 copy-done.2
  127.4 0.0 copy-done.7
  127.4 3.0 %fusion.6 = f32[512,768]{1,0:T(8,128)} fusion(bf16[512,2048]{1,0:T(8,128)(2,1)S(1)} %bitcast.88, bf16[1,2048,768]{2,1,0:T(8,128)(2,1)S(1)} %copy-done.7), kind=kOutput, calls=%fused_computation.12 | convolution fusion | flops 1610612736 | bytes 6815744 | tf_op jit(solution)/shard_map/dot_general | solution.py:28
  130.4 8.3 %fusion.8 = bf16[512,2048]{1,0:T(8,128)(2,1)} fusion(bf16[1,768,2048]{2,1,0:T(8,128)(2,1)S(1)} %copy-done, f32[512,768]{1,0:T(8,128)} %fusion.6, bf16[512,2048]{1,0:T(8,128)(2,1)} %bitcast.89, bf16[1,2048,768]{2,1,0:T(8,128)(2,1)} %param.27), kind=kOutput, calls=%fused_computation.14 | convolution fusion | flops 3224633344 | bytes 12058624 | tf_op jit(solution)/shard_map/dot_general | solution.py:31
  138.7 4.6 %all-to-all-start.1 = ((bf16[4,128,2048]{2,1,0:T(8,128)(2,1)}), bf16[4,128,2048]{2,1,0:T(8,128)(2,1)}, u32[]{:S(2)}, u32[]{:S(2)}) async-start(bf16[4,128,2048]{2,1,0:T(8,128)(2,1)} %bitcast.87), calls=%async_computation.1 | async-start | bytes 4194304 | tf_op jit(solution)/shard_map/all_to_all | solution.py:131
  143.3 0.0 reduce-scatter.3.cloned.1.call-start
  143.4 0.0 copy-done.4
  143.4 1.0 copy.27
  144.4 1.3 reshape.311
  145.8 8.3 %scatter_custom_fusion.1 = f32[512]{0:T(512)S(1)} fusion(s32[2048]{0:T(1024)S(1)} %bitcast.95, f32[2048]{0:T(1024)S(1)} %reshape.311, f32[]{:T(128)} %constant.112.clone.1), kind=kCustom, calls=%fused_computation.134 | custom fusion | bytes 2052 | tf_op jit(solution)/shard_map/scatter | solution.py:118
  154.0 13.5 %all-to-all-done.1 = bf16[4,128,2048]{2,1,0:T(8,128)(2,1)} async-done(((bf16[4,128,2048]{2,1,0:T(8,128)(2,1)}), bf16[4,128,2048]{2,1,0:T(8,128)(2,1)}, u32[]{:S(2)}, u32[]{:S(2)}) %all-to-all-start.1) | async-done | bytes 2097184 | tf_op jit(solution)/shard_map/all_to_all | solution.py:131
  167.5 11.9 %scatter_custom_fusion.2 = f32[1024,2048]{1,0:T(8,128)} fusion(s32[512]{0:T(512)S(1)} %get-tuple-element.11, bf16[512,2048]{1,0:T(8,128)(2,1)} %bitcast.25, f32[]{:T(128)} %constant.112.clone.1, f32[512]{0:T(512)S(1)} %scatter_custom_fusion.1), kind=kCustom, calls=%fused_computation.5 | custom fusion | flops 3145728 | bytes 10487812 | tf_op jit(solution)/shard_map/scatter-add | solution.py:134
  179.4 6.0 %convert_element_type.114 = bf16[1024,2048]{1,0:T(8,128)(2,1)} convert(f32[1024,2048]{1,0:T(8,128)} %scatter_custom_fusion.2) | non-fusion elementwise | flops 2097152 | bytes 12582912 | tf_op jit(solution)/shard_map/convert_element_type | solution.py:137
  185.4 0.0 reduce-scatter.3.cloned.1.call-update
  185.4 1.2 fusion.15
  186.7 0.0 all-gather.4.cloned.1.call-done
  186.7 2.3 convolution_convert_fusion.2
  189.0 0.0 copy-start.3
  189.0 0.6 copy-done.3
  189.6 1.3 collective-permute-start
  191.0 0.8 collective-permute-done
  191.8 0.9 fusion.63
  192.8 0.4 fusion.24
  193.2 0.8 copy-done.1
  194.1 0.0 copy-start.6
  194.1 1.1 broadcast_add_fusion
  195.2 0.1 copy.22
  195.3 0.2 fusion.59
  195.5 0.0 copy-done.8
  195.5 0.2 fusion.35
  195.8 0.1 fusion.33
  195.9 0.0 all-gather.6.cloned.1.call-done
  195.9 2.9 %convolution_convert_fusion.1 = bf16[128,2048]{1,0:T(8,128)(2,1)} fusion(bf16[128,512]{0,1:T(8,128)(2,1)S(1)} %fusion.33, bf16[512,2048]{1,0:T(8,128)(2,1)} %all-gather.6.cloned.1.call-done), kind=kOutput, calls=%fused_computation.15 | convolution fusion | flops 268697600 | bytes 2752512 | tf_op jit(solution)/shard_map/dot_general | solution.py:86
  198.8 35.1 %reduce-scatter.3.cloned.1.call-done = bf16[128,2048]{1,0:T(8,128)(2,1)} async-done(((bf16[1024,2048]{1,0:T(8,128)(2,1)}), bf16[128,2048]{1,0:T(8,128)(2,1)}) %reduce-scatter.3.cloned.1.call-update) | async-done | bytes 524304 | tf_op jit(solution)/shard_map/reduce_scatter | solution.py:136
  233.9 2.1 add_convert_fusion
  (34 shorter events, 0.3 us)
Async XLA Ops:
  7.2 123.2 %copy-start = (bf16[1,768,2048]{2,1,0:T(8,128)(2,1)S(1)}, bf16[1,768,2048]{2,1,0:T(8,128)(2,1)}, u32[]{:S(2)}) copy-start(bf16[1,768,2048]{2,1,0:T(8,128)(2,1)} %param.28) | copy-start | bytes 9437188
  7.2 53.2 %all-gather.8.cloned.1.call-start = ((), (), s32[]{:S(2)}) async-start(), calls=%async_computation.6 | async-start | bytes 4718592 | tf_op jit(solution)/shard_map/all_gather | solution.py:171
  10.7 176.0 %all-gather.4.cloned.1.call-start = ((), (), s32[]{:S(2)}) async-start(), calls=%async_computation.4 | async-start | bytes 2359296 | tf_op jit(solution)/shard_map/all_gather | solution.py:75
  11.4 184.5 %all-gather.6.cloned.1.call-start = ((), (), s32[]{:S(2)}) async-start(), calls=%async_computation.5 | async-start | bytes 2359296 | tf_op jit(solution)/shard_map/all_gather | solution.py:88
  12.2 186.6 %reduce-scatter.5.cloned.1.call-start = ((), (), s32[]{:S(2)}) async-start(), calls=%async_computation.8 | async-start | bytes 4718592 | tf_op jit(solution)/shard_map/reduce_scatter | solution.py:140
  71.0 0.7 copy-start.5
  96.6 30.9 %copy-start.7 = (bf16[1,2048,768]{2,1,0:T(8,128)(2,1)S(1)}, bf16[1,2048,768]{2,1,0:T(8,128)(2,1)}, u32[]{:S(2)}) copy-start(bf16[1,2048,768]{2,1,0:T(8,128)(2,1)} %param.26) | copy-start | bytes 9437188
  126.1 1.3 copy-start.2
  138.7 4.7 %copy-start.4 = (bf16[1024,2]{0,1:T(2,128)(2,1)S(1)}, bf16[1024,2]{0,1:T(2,128)(2,1)}, u32[]{:S(2)}) copy-start(bf16[1024,2]{0,1:T(2,128)(2,1)} %param.25) | copy-start | bytes 12292
  138.7 28.8 %all-to-all-start.1 = ((bf16[4,128,2048]{2,1,0:T(8,128)(2,1)}), bf16[4,128,2048]{2,1,0:T(8,128)(2,1)}, u32[]{:S(2)}, u32[]{:S(2)}) async-start(bf16[4,128,2048]{2,1,0:T(8,128)(2,1)} %bitcast.87), calls=%async_computation.1 | async-start | bytes 4194304 | tf_op jit(solution)/shard_map/all_to_all | solution.py:131
  143.3 90.6 %reduce-scatter.3.cloned.1.call-start = ((), (), s32[]{:S(2)}) async-start(), calls=%async_computation.7 | async-start | bytes 4718592 | tf_op jit(solution)/shard_map/reduce_scatter | solution.py:136
  185.4 1.3 copy-start.9
  189.0 0.7 copy-start.3
  189.6 2.1 collective-permute-start
  193.2 0.8 copy-start.1
  194.0 1.5 copy-start.8
  194.1 1.7 copy-start.6
Sparse Core Ops, SparseCore 0:
  10.8 49.5 all-gather.7
  62.0 27.9 all-gather.3
  91.6 29.9 all-gather.5
  123.8 48.8 reduce-scatter.4
  185.5 48.2 reduce-scatter.2
where the time goes:
time: 243 us
  waiting for transfers between devices  99 us (41%)
  local copies, waits for them, and re-layouts  35.5 us (15%)
  other arithmetic  31 us (13%)
  blocking collectives  29.5 us (12%)
  matrix products  27.2 us (11%)
  between operations  14.1 us (6%)
  starting transfers between devices  6.07 us (2%)
    all_gather x1, waiting for transfers between devices, shards(): lax.all_gather(moe_normed, 'tp', axis=0, tiled=True)  48.2 us
    reduce_scatter x1, waiting for transfers between devices, expert_half(): lax.psum_scatter(routed.astype(jnp.bfloat16), 'tp', scatter_dimension=0,...  35.1 us
    all_to_all x1, blocking collectives, expert_half(): lax.all_to_all(outgoing, 'ep', split_axis=0, concat_axis=0, tiled=True)  29.5 us
    all_to_all x1, waiting for transfers between devices, expert_half(): lax.all_to_all(results, 'ep', split_axis=0, concat_axis=0, tiled=True)  13.5 us
    scatter-add x1, other arithmetic, expert_half(): jnp.zeros((block_rows, model_width), jnp.float32).at[slot_token]  11.9 us
    dot_general x1, matrix products, expert_ffn(): jnp.dot(hidden, w_down, preferred_element_type=jnp.float32)  8.29 us
    scatter x1, local copies, waits for them, and re-layouts, expert_half(): jnp.zeros((ep_count * capacity,), jnp.float32).at[slot_index]  8.25 us
    scatter x1, local copies, waits for them, and re-layouts, expert_half(): slot_token = jnp.full((ep_count * capacity,), block_rows, jnp.int32).at[s...  8.04 us
  transfers between devices with their start and end apart: 7, of which 4 were waited for; matrix products, arithmetic and copies ran while one was open for 35% of the time, Pallas kernels for 0%

commit v1 on v0

v1 whole, which is shorter than its diff:
```python
import functools

import jax
import jax.numpy as jnp
from jax import lax
from jax.experimental import pallas as pl
from jax.experimental.pallas import tpu as pltpu
from jax.sharding import PartitionSpec as P

SEQS_MIX = 1
CORES = 2

NORM_EPS = 1e-06
ROUTED_SCALE = 2.5
MESH = pl.DeviceIdType.MESH


def rms_rows(values, gain):
    floats = values.astype(jnp.float32)
    scaled = floats * lax.rsqrt(jnp.mean(floats * floats, axis=-1, keepdims=True) + NORM_EPS)
    return (scaled * gain).astype(jnp.bfloat16)


def remote(src, dst, send_sem, recv_sem, device):
    return pltpu.make_async_remote_copy(
        src_ref=src,
        dst_ref=dst,
        send_sem=send_sem,
        recv_sem=recv_sem,
        device_id=device,
        device_id_type=MESH,
    )


def greet(devices):
    barrier = pltpu.get_barrier_semaphore()
    for device in devices:
        pl.semaphore_signal(barrier, inc=1, device_id=device, device_id_type=MESH)
    pl.semaphore_wait(barrier, len(devices))


class Place:
    def __init__(self, ep_count, tp_count):
        self.ep_count, self.tp_count = ep_count, tp_count
        self.chips = tp_count // CORES
        self.far = self.chips // 2
        self.ep, self.tp = lax.axis_index("ep"), lax.axis_index("tp")
        self.chip, self.core = self.tp // CORES, self.tp % CORES

    def at(self, step):
        return (self.chip + step + self.chips) % self.chips

    def column(self, step, core):
        return self.at(step) * CORES + core

    def side(self, way):
        return (self.ep, self.column(1 if way == 0 else -1, self.core))

    def sibling(self):
        return (self.ep, self.column(0, 1 - self.core))

    def peers(self):
        return [((self.ep + i) % self.ep_count, self.tp) for i in range(1, self.ep_count)]


def ring_keys(chips):
    far = chips // 2
    return [
        (way, dist, half)
        for dist in range(1, far + 1)
        for turn in range(2)
        for way, half in ((0, turn), (1, 1 - turn))
        if dist < far or half == way
    ]


class RingGather:
    def __init__(self, place, buf, send, recv):
        self.place, self.buf, self.send, self.recv = place, buf, send, recv
        self.rows = buf.shape[1] // 2
        self.keys = ring_keys(place.chips)
        self.started = []

    def view(self, step, core, half):
        return self.buf.at[self.place.column(step, core), pl.ds(half * self.rows, self.rows)]

    def push(self, key):
        way, dist, half = key
        n = self.keys.index(key)
        block = self.view(-(dist - 1) if way == 0 else dist - 1, self.place.core, half)
        self._go(block, n, self.place.side(way))

    def _go(self, block, n, device):
        copy = remote(block, block, self.send.at[n], self.recv.at[n], device)
        copy.start()
        self.started.append(copy)

    def _arrived(self, block, n, device):
        remote(block, block, self.send.at[n], self.recv.at[n], device).wait_recv()

    def start(self):
        for key in self.keys:
            if key[1] == 1:
                self.push(key)
        block = self.buf.at[self.place.tp]
        self._go(block, 2 * len(self.keys), self.place.sibling())

    def step(self, dist):
        for n, key in enumerate(self.keys):
            if key[1] != dist:
                continue
            way, _, half = key
            block = self.view(-dist if way == 0 else dist, self.place.core, half)
            self._arrived(block, n, self.place.side(way))
            if (way, dist + 1, half) in self.keys:
                self.push((way, dist + 1, half))
            self._go(block, len(self.keys) + n, self.place.sibling())

    def arrive(self):
        for n, (way, dist, half) in enumerate(self.keys):
            block = self.view(-dist if way == 0 else dist, 1 - self.place.core, half)
            self._arrived(block, len(self.keys) + n, self.place.sibling())
        block = self.buf.at[self.place.column(0, 1 - self.place.core)]
        self._arrived(block, 2 * len(self.keys), self.place.sibling())

    def close(self):
        for copy in self.started:
            copy.wait_send()


def dispatch_kernel(
    ep_count, tp_count, moe_in, gain, table, gate_up, down, w_in, w_out,
    received, shared, w_in_all, w_out_all,
    rows_all, outgoing,
    xs, xr, ins, inr, outs, outr, as_, ar,
):
    place = Place(ep_count, tp_count)
    greet([place.side(0), place.side(1), place.sibling()] + place.peers())
    me = place.tp
    rows, width = moe_in.shape
    rows_all[pl.ds(me, 1)] = rms_rows(moe_in[...], gain[...])[None]
    tokens = RingGather(place, rows_all, xs, xr)
    tokens.start()
    w_in_all[pl.ds(me, 1)] = w_in[...][None]
    w_out_all[pl.ds(me, 1)] = w_out[...][None]
    for dist in range(1, place.far + 1):
        tokens.step(dist)
    first = RingGather(place, w_in_all, ins, inr)
    second = RingGather(place, w_out_all, outs, outr)
    tokens.arrive()
    first.start()
    second.start()

    cut = 512
    slots = table.shape[0]
    capacity = slots // ep_count

    def pick(i, carry):
        columns = pl.ds(pl.multiple_of(i * cut, cut), cut)
        block = rows_all[:, :, columns].reshape(tp_count * rows, cut)
        picked = jnp.dot(table[...], block, preferred_element_type=jnp.float32)
        outgoing[:, :, columns] = picked.astype(jnp.bfloat16).reshape(ep_count, capacity, cut)
        return carry

    lax.fori_loop(0, width // cut, pick, 0)
    copies = []
    for i, (peer, column) in enumerate(place.peers()):
        copy = remote(
            outgoing.at[peer], received.at[place.ep], as_.at[i], ar.at[i], (peer, column)
        )
        copy.start()
        copies.append(copy)
    received[pl.ds(place.ep, 1)] = outgoing[pl.ds(place.ep, 1)]
    for dist in range(1, place.far + 1):
        first.step(dist)

    units = down.shape[0]

    def ffn(i, carry):
        block = rows_all[pl.ds(i * CORES, CORES)].reshape(CORES * rows, width)
        both = lax.dot_general(
            block, gate_up[...], (((1,), (1,)), ((), ())), preferred_element_type=jnp.float32
        )
        spread = both.shape[1] // 2
        hidden = (jax.nn.silu(both[:, :spread]) * both[:, spread:]).astype(jnp.bfloat16)
        result = jnp.dot(hidden, down[...], preferred_element_type=jnp.float32)
        shared[pl.ds(i * CORES, CORES)] = result.astype(jnp.bfloat16).reshape(CORES, rows, width)
        return carry

    lax.fori_loop(0, tp_count // CORES, ffn, 0)
    for dist in range(1, place.far + 1):
        second.step(dist)
    first.arrive()
    second.arrive()
    for i in range(1, ep_count):
        source = (place.ep - i + ep_count) % ep_count
        remote(
            received.at[source], received.at[source], as_.at[i - 1], ar.at[i - 1],
            (source, place.tp),
        ).wait_recv()
    for copy in copies:
        copy.wait_send()
    for gather in (tokens, first, second):
        gather.close()


def combine_kernel(
    ep_count, tp_count, seq_len, results, table, shared, mix_in, mix_gain, w_in, pool_mat,
    pool_scale, w_out,
    mixed, moe_out,
    returned, own, for_sibling, from_sibling, sums, arrived, tail, prior,
    as_, ar, hs, hr, ss, sr, rs, rr,
):
    place = Place(ep_count, tp_count)
    devices = ep_count * tp_count
    flat = place.ep * tp_count + place.tp
    after, before = (flat + 1) % devices, (flat + devices - 1) % devices
    after = (after // tp_count, after % tp_count)
    before = (before // tp_count, before % tp_count)
    greet([place.side(0), place.side(1), place.sibling(), after, before] + place.peers())
    copies = []
    for i, (peer, column) in enumerate(place.peers()):
        copy = remote(
            results.at[peer], returned.at[place.ep], as_.at[i], ar.at[i], (peer, column)
        )
        copy.start()
        copies.append(copy)
    returned[pl.ds(place.ep, 1)] = results[pl.ds(place.ep, 1)]

    rows, width = mix_in.shape
    groups, group_ch = pool_mat.shape[0], pool_mat.shape[1]
    reach = 2**groups
    normed = rms_rows(mix_in[...], mix_gain[...])
    projected = jnp.dot(
        normed, w_in[...].reshape(width, groups * group_ch), preferred_element_type=jnp.float32
    ).astype(jnp.bfloat16)
    tail[...] = projected[rows - reach :]
    halo = remote(tail, prior, hs, hr, after)
    halo.start()
    halo.wait()
    first_row = flat * rows
    keep = jnp.where(first_row % seq_len == 0, 0.0, 1.0)
    extended = jnp.concatenate(
        [prior[...].astype(jnp.float32) * keep, projected.astype(jnp.float32)], axis=0
    )
    position = (first_row + lax.broadcasted_iota(jnp.int32, (rows, group_ch), 0)) % seq_len
    pieces = []
    for group in range(groups):
        channels = slice(group * group_ch, (group + 1) * group_ch)
        running = extended[:, channels]
        for level in range(group + 1):
            running = running + pltpu.roll(running, 2**level, 0)
        counts = jnp.minimum(position + 1, 2 ** (group + 1)).astype(jnp.float32)
        pooled = (running[reach:] / counts - extended[reach:, channels]).astype(jnp.bfloat16)
        grouped = jnp.dot(pooled, pool_mat[group], preferred_element_type=jnp.float32)
        pieces.append((grouped * pool_scale[:, channels]).astype(jnp.bfloat16))
    pool_out = jnp.concatenate(pieces, axis=1)
    span = w_out.shape[2]
    for column in range(tp_count):
        mixed[:, column * span : (column + 1) * span] = jnp.dot(
            pool_out, w_out[column], preferred_element_type=jnp.float32
        ).astype(jnp.bfloat16)

    for i in range(1, ep_count):
        source = (place.ep - i + ep_count) % ep_count
        remote(
            returned.at[source], returned.at[source], as_.at[i - 1], ar.at[i - 1],
            (source, place.tp),
        ).wait_recv()

    slots = table.shape[2]
    order = [place.far]
    for dist in range(place.far - 1, 0, -1):
        order += [dist, -dist]
    order += [0]
    cut = 512

    def total(step):
        chip = place.at(step)
        block = table[pl.ds(chip * CORES, CORES)].reshape(CORES * rows, slots)

        def part(i, carry):
            columns = pl.ds(pl.multiple_of(i * cut, cut), cut)
            values = jnp.dot(
                block,
                returned[:, :, columns].reshape(slots, cut),
                preferred_element_type=jnp.float32,
            ).reshape(CORES, rows, cut)
            values = values + shared[pl.ds(chip * CORES, CORES), :, columns].astype(jnp.float32)
            mine = jnp.where(place.core == 0, 1.0, 0.0)
            low, high = values[0], values[1]
            own[pl.ds(chip, 1), :, columns] = (low * mine + high * (1.0 - mine))[None]
            other = low * (1.0 - mine) + high * mine
            for_sibling[pl.ds(chip, 1), :, columns] = other.astype(jnp.bfloat16)[None]
            return carry

        lax.fori_loop(0, width // cut, part, 0)

    half_rows = rows // 2
    keys = ring_keys(place.chips)
    moves = []
    for n, step in enumerate(order):
        total(step)
        chip = place.at(step)
        copy = remote(
            for_sibling.at[chip], from_sibling.at[chip], ss.at[n], sr.at[n], place.sibling()
        )
        copy.start()
        moves.append(copy)

    def landed(key):
        way, dist, half = key
        n = keys.index(key)
        block = arrived.at[n]
        remote(block, block, rs.at[n], rr.at[n], place.side(way)).wait_recv()
        return arrived[n].astype(jnp.float32)

    for n, step in enumerate(order):
        chip = place.at(step)
        block = from_sibling.at[chip]
        remote(block, block, ss.at[n], sr.at[n], place.sibling()).wait_recv()
        dist = abs(step)
        if dist == 0:
            continue
        ways = (0, 1) if dist == place.far else ((0,) if step > 0 else (1,))
        for way, d, half in keys:
            if d != dist or way not in ways:
                continue
            span_rows = pl.ds(half * half_rows, half_rows)
            value = own[pl.ds(chip, 1), span_rows] + from_sibling[
                pl.ds(chip, 1), span_rows
            ].astype(jnp.float32)
            if (way, dist + 1, half) in keys:
                value = value + landed((way, dist + 1, half))[None]
            k = keys.index((way, dist, half))
            sums[pl.ds(k, 1)] = value.astype(jnp.bfloat16)
            copy = remote(sums.at[k], arrived.at[k], rs.at[k], rr.at[k], place.side(way))
            copy.start()
            moves.append(copy)
    for half in range(2):
        span_rows = pl.ds(half * half_rows, half_rows)
        value = own[pl.ds(place.chip, 1), span_rows] + from_sibling[
            pl.ds(place.chip, 1), span_rows
        ].astype(jnp.float32)
        value = value[0]
        for way in range(2):
            if (way, 1, half) in keys:
                value = value + landed((way, 1, half))
        moe_out[half * half_rows : (half + 1) * half_rows, :] = value.astype(jnp.bfloat16)
    for copy in copies + moves:
        copy.wait_send()


def vmem(count):
    return [pl.BlockSpec(memory_space=pltpu.VMEM)] * count


def shards(
    mix_in, mix_gain, mix_w_in, pool_mat, pool_scale, mix_w_out, moe_in, moe_gain, routes,
    route_score, exp_gate, exp_up, exp_down, shared_gate, shared_up, shared_down,
):
    ep_count, tp_count = lax.axis_size("ep"), lax.axis_size("tp")
    rows, width = moe_in.shape
    block_rows, top_count = routes.shape
    capacity = 2 * block_rows * top_count // (ep_count * tp_count)
    slots = ep_count * capacity
    dma = lambda n: pltpu.SemaphoreType.DMA((n,))
    bf16 = jnp.bfloat16
    messages = len(ring_keys(tp_count // CORES))

    column = lax.axis_index("tp")
    scores = route_score.astype(jnp.float32)
    weights = scores / jnp.sum(scores, axis=1, keepdims=True) * ROUTED_SCALE
    names = lax.iota(jnp.int32, ep_count) * tp_count + column
    hit = routes[:, :, None] == names[None, None, :]
    named = jnp.any(hit, axis=1)
    weight = jnp.sum(jnp.where(hit, weights[:, :, None], 0.0), axis=1)
    counted = named.astype(jnp.int32)
    spot = jnp.where(named, jnp.cumsum(counted, axis=0) - counted, -1)
    slot = lax.iota(jnp.int32, capacity)
    pick_table = (
        (spot.T[:, None, :] == slot[None, :, None]).astype(bf16).reshape(slots, block_rows)
    )
    sum_table = jnp.where(
        spot[:, :, None] == slot[None, None, :], weight[:, :, None], 0.0
    ).astype(bf16).reshape(tp_count, rows, slots)
    units = shared_gate.shape[0]
    spread = -(-units // 128) * 128
    pad = ((0, spread - units), (0, 0))
    gate_up = jnp.concatenate([jnp.pad(shared_gate, pad), jnp.pad(shared_up, pad)], axis=0)
    down = jnp.pad(shared_down, pad)

    received, shared, w_in_all, w_out_all = pl.pallas_call(
        functools.partial(dispatch_kernel, ep_count, tp_count),
        out_shape=[
            jax.ShapeDtypeStruct((ep_count, capacity, width), bf16),
            jax.ShapeDtypeStruct((tp_count, rows, width), bf16),
            jax.ShapeDtypeStruct((tp_count,) + mix_w_in.shape, bf16),
            jax.ShapeDtypeStruct((tp_count,) + mix_w_out.shape, bf16),
        ],
        in_specs=vmem(7),
        out_specs=vmem(4),
        scratch_shapes=[
            pltpu.VMEM((tp_count, rows, width), bf16),
            pltpu.VMEM((ep_count, capacity, width), bf16),
        ]
        + [dma(2 * messages + 1) for _ in range(6)]
        + [dma(ep_count - 1) for _ in range(2)],
        compiler_params=pltpu.CompilerParams(collective_id=0, has_side_effects=True),
    )(moe_in, moe_gain[None, :], pick_table, gate_up, down, mix_w_in, mix_w_out)

    flat_rows = received.reshape(slots, width)
    gate_act = jnp.dot(flat_rows, exp_gate[0], preferred_element_type=jnp.float32)
    up_act = jnp.dot(flat_rows, exp_up[0], preferred_element_type=jnp.float32)
    hidden = (jax.nn.silu(gate_act) * up_act).astype(bf16)
    results = jnp.dot(hidden, exp_down[0], preferred_element_type=jnp.float32).astype(bf16)

    chips = tp_count // CORES
    reach = 2 ** pool_mat.shape[0]
    channels = mix_w_in.shape[1]
    seq_len = mix_in.shape[0] * ep_count * tp_count // SEQS_MIX
    mixed, moe_out = pl.pallas_call(
        functools.partial(combine_kernel, ep_count, tp_count, seq_len),
        out_shape=[
            jax.ShapeDtypeStruct(mix_in.shape, bf16),
            jax.ShapeDtypeStruct(moe_in.shape, bf16),
        ],
        in_specs=vmem(9),
        out_specs=vmem(2),
        scratch_shapes=[
            pltpu.VMEM((ep_count, capacity, width), bf16),
            pltpu.VMEM((chips, rows, width), jnp.float32),
            pltpu.VMEM((chips, rows, width), bf16),
            pltpu.VMEM((chips, rows, width), bf16),
            pltpu.VMEM((messages, rows // 2, width), bf16),
            pltpu.VMEM((messages, rows // 2, width), bf16),
            pltpu.VMEM((reach, channels), bf16),
            pltpu.VMEM((reach, channels), bf16),
            dma(ep_count - 1),
            dma(ep_count - 1),
            pltpu.SemaphoreType.DMA,
            pltpu.SemaphoreType.DMA,
            dma(chips),
            dma(chips),
            dma(messages),
            dma(messages),
        ],
        compiler_params=pltpu.CompilerParams(collective_id=1, has_side_effects=True),
    )(
        results.reshape(ep_count, capacity, width), sum_table, shared, mix_in,
        mix_gain[None, :], w_in_all, pool_mat, pool_scale[None, :], w_out_all,
    )
    return (mixed, moe_out)


def solution(mesh):
    return jax.shard_map(
        shards,
        mesh=mesh,
        in_specs=(
            P(("ep", "tp"), None),
            P(),
            P("tp", None),
            P(),
            P(),
            P(None, "tp"),
            P(("ep", "tp"), None),
            P(),
            P("ep", None),
            P("ep", None),
            P(("ep", "tp"), None, None),
            P(("ep", "tp"), None, None),
            P(("ep", "tp"), None, None),
            P("tp", None),
            P("tp", None),
            P("tp", None),
        ),
        out_specs=(P(("ep", "tp"), None), P(("ep", "tp"), None)),
        check_vma=False,
    )
```

time: 243 us -> 215 us (0.88)
  Pallas kernels: 0 us -> 166 us
  waiting for transfers between devices: 99 us -> 0 us
  blocking collectives: 29.5 us -> 0 us
  other arithmetic: 31 us -> 12.9 us
  local copies, waits for them, and re-layouts: 35.5 us -> 20.8 us
  matrix products: 27.2 us -> 13.8 us
  between operations: 14.1 us -> 0.76 us
  starting transfers between devices: 6.07 us -> 0 us
    pallas_call x0 -> x2, Pallas kernels: none -> 166 us  [the longest x1 92 us: shards(): pl.pallas_call(functools.partial(dispatch_kernel, ep_count, tp_count), ou...]
    all_gather x3 -> x0, waiting for transfers between devices: 48.3 us -> none  [the longest x1 48.2 us: shards(): lax.all_gather(moe_normed, 'tp', axis=0, tiled=True)]
    reduce_scatter x2 -> x0, waiting for transfers between devices: 35.1 us -> none  [the longest x1 35.1 us: expert_half(): lax.psum_scatter(routed.astype(jnp.bfloat16), 'tp', scatter_dimension=0,...]
    all_to_all x1 -> x0, blocking collectives: 29.5 us -> none  [expert_half(): lax.all_to_all(outgoing, 'ep', split_axis=0, concat_axis=0, tiled=True)]
    scatter x2 -> x0, local copies, waits for them, and re-layouts: 16.3 us -> none  [the longest x1 8.25 us: expert_half(): jnp.zeros((ep_count * capacity,), jnp.float32).at[slot_index]]
    all_to_all x1 -> x0, waiting for transfers between devices: 13.5 us -> none  [expert_half(): lax.all_to_all(results, 'ep', split_axis=0, concat_axis=0, tiled=True)]
    dot_general x7 -> x2, matrix products: 27.2 us -> 13.8 us  [the longest x1 8.33 us: shards(): jnp.dot(hidden, exp_down[0], preferred_element_type=jnp.float32)]
    scatter-add x1 -> x0, other arithmetic: 11.9 us -> none  [expert_half(): jnp.zeros((block_rows, model_width), jnp.float32).at[slot_token]]
  transfers between devices with their start and end apart: 7 -> 0, of which waited for: 4 -> 0; matrix products, arithmetic and copies ran while one was open for 35% -> 0% of each run, Pallas kernels for 0% -> 0%
where the time goes in v1:
time: 215 us
  Pallas kernels  166 us (77%)
  local copies, waits for them, and re-layouts  20.8 us (10%)
  matrix products  13.8 us (6%)
  other arithmetic  12.9 us (6%)
    pallas_call x1, Pallas kernels, shards(): pl.pallas_call(functools.partial(dispatch_kernel, ep_count, tp_count), ou...  92 us
    pallas_call x1, Pallas kernels, shards(): pl.pallas_call(functools.partial(combine_kernel, ep_count, tp_count, seq_...  74.2 us
    dot_general x1, matrix products, shards(): jnp.dot(hidden, exp_down[0], preferred_element_type=jnp.float32)  8.33 us
    eq x2, local copies, waits for them, and re-layouts, shards(): spot[:, :, None] == slot[None, None, :]  7.98 us
    unnamed x25, local copies, waits for them, and re-layouts  5.58 us
    dot_general x1, matrix products, shards(): jnp.dot(flat_rows, exp_gate[0], preferred_element_type=jnp.float32)  5.51 us
    broadcast_in_dim x2, local copies, waits for them, and re-layouts, shards(): jnp.where(spot[:, :, None] == slot[None, None, :], weight[:, :, None], 0.0)  4.33 us

profile of v1, /device:TPU:0, one launch (start us, length us, event | category | flops | bytes accessed | tf_op | source)
XLA Modules:
  0.0 214.6 jit_solution(101062961393614212)
XLA Ops:
  0.6 0.0 copy-start
  0.6 0.0 copy-start.1
  0.7 0.0 copy-start.9
  0.7 0.6 copy-done.9
  1.3 0.8 compare_reduce_fusion
  2.1 0.0 copy-start.3
  2.1 0.6 copy.31
  2.7 0.0 copy-done.3
  2.7 2.2 %reduce-window.6 = s32[4,8,128]{2,1,0:T(8,128)S(1)} reduce-window(s32[4,8,128]{2,1,0:T(8,128)} %bitcast.53, s32[]{:T(128)} %constant.7.clone.1), window={size=1x1x128 pad=0_0x0_0x127_0}, to_apply=%region_1.0 | reduce-window | flops 520192 | bytes 32772 | tf_op jit(solution)/shard_map/reduce-window
  4.9 0.0 copy-start.2
  4.9 0.8 slice_reduce_fusion
  5.7 1.4 reduce-window.9
  7.2 0.0 copy-done.2
  7.2 0.8 add_bitcast_fusion
  8.0 0.7 fusion.18
  8.7 0.0 copy-start.6
  8.7 0.6 copy-done.6
  9.3 1.3 fusion.9.table
  10.6 2.2 %fusion.14.gate_up = bf16[256,2048]{1,0:T(8,128)(2,1)} fusion(bf16[96,2048]{1,0:T(8,128)(2,1)} %param.30, bf16[96,2048]{1,0:T(8,128)(2,1)} %param.29), kind=kLoop, calls=%fused_computation.15 | loop fusion | flops 4194304 | bytes 1835008 | tf_op jit(solution)/shard_map/concatenate | solution.py:390
  12.8 0.0 copy-done.1
  12.8 0.8 pad.12.down
  13.6 92.0 %shard_map.167 = (bf16[4,128,2048]{2,1,0:T(8,128)(2,1)}, bf16[8,128,2048]{2,1,0:T(8,128)(2,1)}, bf16[8,256,512]{2,1,0:T(8,128)(2,1)}, bf16[8,512,256]{2,1,0:T(8,128)(2,1)}) custom-call(bf16[128,2048]{1,0:T(8,128)(2,1)} %moe_in.1, f32[1,2048]{1,0:T(1,128)} %bitcast.54, bf16[512,1024]{1,0:T(8,128)(2,1)} %fusion.9.table, bf16[256,2048]{1,0:T(8,128)(2,1)} %fusion.14.gate_up, ...), custom_call_target="tpu_custom_call" | custom-call | tf_op jit(solution)/shard_map/pallas_call | solution.py:393
  105.6 5.5 %fusion.4 = f32[512,768]{1,0:T(8,128)} fusion(bf16[512,2048]{1,0:T(8,128)(2,1)} %bitcast.58, bf16[1,2048,768]{2,1,0:T(8,128)(2,1)} %param.26), kind=kOutput, calls=%fused_computation.4 | convolution fusion | flops 1610612736 | bytes 6815744 | tf_op jit(solution)/shard_map/dot_general | solution.py:413
  111.2 0.0 copy-done
  111.2 0.0 copy-start.4
  111.2 8.3 %fusion.6 = bf16[512,2048]{1,0:T(8,128)(2,1)} fusion(bf16[1,768,2048]{2,1,0:T(8,128)(2,1)S(1)} %copy-done, f32[512,768]{1,0:T(8,128)} %fusion.4, bf16[512,2048]{1,0:T(8,128)(2,1)} %bitcast.59, bf16[1,2048,768]{2,1,0:T(8,128)(2,1)} %param.27), kind=kOutput, calls=%fused_computation.6 | convolution fusion | flops 3224633344 | bytes 12058624 | tf_op jit(solution)/shard_map/dot_general | solution.py:416
  119.5 0.0 copy-done.4
  119.5 1.0 copy.24
  120.5 4.9 %eq.62 = s32[1024,4,128]{2,1,0:T(4,128)} broadcast(s32[1024,4]{1,0:T(8,128)} %copy.24), dimensions={0,1} | broadcast | bytes 2113536 | tf_op jit(solution)/shard_map/eq | solution.py:385
  125.4 0.0 copy-start.8
  125.4 0.0 copy-start.5
  125.4 0.0 copy-start.10
  125.4 3.1 %eq.63 = s32[8,128,512]{2,1,0:T(8,128)} reshape(s32[1024,4,128]{2,1,0:T(4,128)} %eq.62) | data formatting | bytes 4194304 | tf_op jit(solution)/shard_map/eq | solution.py:385
  128.5 0.0 copy-done.8
  128.5 0.0 copy-start.7
  128.6 0.0 copy-done.5
  128.6 0.0 copy-done.10
  128.6 0.1 fusion.17
  128.7 0.2 copy.25
  128.9 2.0 broadcast_in_dim.55
  130.9 2.3 %broadcast_in_dim.56 = bf16[8,128,512]{2,1,0:T(8,128)(2,1)} reshape(bf16[1024,4,128]{2,1,0:T(4,128)(2,1)} %broadcast_in_dim.55) | data formatting | bytes 2097152 | tf_op jit(solution)/shard_map/jit(_where)/broadcast_in_dim | solution.py:384
  133.2 0.0 copy-done.7
  133.2 3.3 %select_convert_fusion.table = bf16[8,128,512]{2,1,0:T(8,128)(2,1)} fusion(bf16[8,128,512]{2,1,0:T(8,128)(2,1)} %broadcast_in_dim.56, s32[8,128,512]{2,1,0:T(8,128)} %eq.63, s32[512]{0:T(512)S(1)} %copy-done.7), kind=kLoop, calls=%fused_computation.10 | loop fusion | flops 1048576 | bytes 4196352 | tf_op jit(solution)/shard_map/convert_element_type | solution.py:386
  136.5 74.2 %shard_map.168 = (bf16[128,2048]{1,0:T(8,128)(2,1)}, bf16[128,2048]{1,0:T(8,128)(2,1)}) custom-call(bf16[4,128,2048]{2,1,0:T(8,128)(2,1)} %bitcast.52, bf16[8,128,512]{2,1,0:T(8,128)(2,1)} %select_convert_fusion.table, bf16[8,128,2048]{2,1,0:T(8,128)(2,1)} %get-tuple-element.7.shared, bf16[128,2048]{1,0:T(8,128)(2,1)} %mix_in.1, f32[1,2048]{1,0:T(1,128)} %bitcast.56, ...), custom_call_target="tpu_custom_call" | custom-call | tf_op jit(solution)/shard_map/pallas_call | solution.py:422
  210.8 1.9 copy.34
  212.7 1.9 copy.35
  (6 shorter events, 0.1 us)
Async XLA Ops:
  0.6 110.5 %copy-start = (bf16[1,768,2048]{2,1,0:T(8,128)(2,1)S(1)}, bf16[1,768,2048]{2,1,0:T(8,128)(2,1)}, u32[]{:S(2)}) copy-start(bf16[1,768,2048]{2,1,0:T(8,128)(2,1)} %param.28) | copy-start | bytes 9437188
  0.6 12.1 %copy-start.1 = (bf16[96,2048]{1,0:T(8,128)(2,1)S(1)}, bf16[96,2048]{1,0:T(8,128)(2,1)}, u32[]{:S(2)}) copy-start(bf16[96,2048]{1,0:T(8,128)(2,1)} %param.31) | copy-start | bytes 1179652
  0.7 0.6 copy-start.9
  2.1 0.6 copy-start.3
  4.9 2.3 %copy-start.2 = (s32[4,8,128]{2,1,0:T(8,128)}, s32[4,8,128]{2,1,0:T(8,128)S(1)}, u32[]{:S(2)}) copy-start(s32[4,8,128]{2,1,0:T(8,128)S(1)} %reduce-window.6) | copy-start | bytes 49156
  8.7 0.6 copy-start.6
  111.2 8.3 %copy-start.4 = (pred[1024,4]{0,1:T(4,128)(4,1)S(1)}, pred[1024,4]{0,1:T(4,128)(4,1)}, u32[]{:S(2)}) copy-start(pred[1024,4]{0,1:T(4,128)(4,1)} %copy-done.3) | copy-start | bytes 12292
  125.4 3.1 %copy-start.8 = (bf16[1024,2]{0,1:T(2,128)(2,1)S(1)}, bf16[1024,2]{0,1:T(2,128)(2,1)}, u32[]{:S(2)}) copy-start(bf16[1024,2]{0,1:T(2,128)(2,1)} %param.25) | copy-start | bytes 12292
  125.4 3.1 %copy-start.5 = (s32[1024,2]{0,1:T(2,128)S(1)}, s32[1024,2]{0,1:T(2,128)}, u32[]{:S(2)}) copy-start(s32[1024,2]{0,1:T(2,128)} %param.24) | copy-start | bytes 24580
  125.4 3.1 %copy-start.10 = (s32[4]{0:T(128)S(1)}, s32[4]{0:T(128)}, u32[]{:S(2)}) copy-start(s32[4]{0:T(128)} %copy-done.9) | copy-start | bytes 52
  128.5 4.7 %copy-start.7 = (s32[512]{0:T(512)S(1)}, s32[512]{0:T(512)}, u32[]{:S(2)}) copy-start(s32[512]{0:T(512)} %copy-done.6) | copy-start | bytes 6148

commit v2 on v1

v2 whole, which is shorter than its diff:
```python
import functools

import jax
import jax.numpy as jnp
from jax import lax
from jax.experimental import pallas as pl
from jax.experimental.pallas import tpu as pltpu
from jax.sharding import PartitionSpec as P

SEQS_MIX = 1
CORES = 2

NORM_EPS = 1e-06
ROUTED_SCALE = 2.5
MESH = pl.DeviceIdType.MESH


def rms_rows(values, gain):
    floats = values.astype(jnp.float32)
    scaled = floats * lax.rsqrt(jnp.mean(floats * floats, axis=-1, keepdims=True) + NORM_EPS)
    return (scaled * gain).astype(jnp.bfloat16)


def remote(src, dst, send_sem, recv_sem, device):
    return pltpu.make_async_remote_copy(
        src_ref=src,
        dst_ref=dst,
        send_sem=send_sem,
        recv_sem=recv_sem,
        device_id=device,
        device_id_type=MESH,
    )


def greet(devices):
    barrier = pltpu.get_barrier_semaphore()
    for device in devices:
        pl.semaphore_signal(barrier, inc=1, device_id=device, device_id_type=MESH)
    pl.semaphore_wait(barrier, len(devices))


class Place:
    def __init__(self, ep_count, tp_count):
        self.ep_count, self.tp_count = ep_count, tp_count
        self.chips = tp_count // CORES
        self.far = self.chips // 2
        self.ep, self.tp = lax.axis_index("ep"), lax.axis_index("tp")
        self.chip, self.core = self.tp // CORES, self.tp % CORES

    def at(self, step):
        return (self.chip + step + self.chips) % self.chips

    def column(self, step, core):
        return self.at(step) * CORES + core

    def side(self, way):
        return (self.ep, self.column(1 if way == 0 else -1, self.core))

    def sibling(self):
        return (self.ep, self.column(0, 1 - self.core))

    def peers(self):
        return [((self.ep + i) % self.ep_count, self.tp) for i in range(1, self.ep_count)]


def ring_keys(chips):
    far = chips // 2
    return [
        (way, dist, half)
        for dist in range(1, far + 1)
        for turn in range(2)
        for way, half in ((0, turn), (1, 1 - turn))
        if dist < far or half == way
    ]


class RingGather:
    def __init__(self, place, buf, send, recv):
        self.place, self.buf, self.send, self.recv = place, buf, send, recv
        self.rows = buf.shape[1] // 2
        self.keys = ring_keys(place.chips)
        self.started = []

    def view(self, step, core, half):
        return self.buf.at[self.place.column(step, core), pl.ds(half * self.rows, self.rows)]

    def push(self, key):
        way, dist, half = key
        n = self.keys.index(key)
        block = self.view(-(dist - 1) if way == 0 else dist - 1, self.place.core, half)
        self._go(block, n, self.place.side(way))

    def _go(self, block, n, device):
        copy = remote(block, block, self.send.at[n], self.recv.at[n], device)
        copy.start()
        self.started.append(copy)

    def _arrived(self, block, n, device):
        remote(block, block, self.send.at[n], self.recv.at[n], device).wait_recv()

    def start(self):
        for key in self.keys:
            if key[1] == 1:
                self.push(key)
        block = self.buf.at[self.place.tp]
        self._go(block, 2 * len(self.keys), self.place.sibling())

    def step(self, dist):
        for n, key in enumerate(self.keys):
            if key[1] != dist:
                continue
            way, _, half = key
            block = self.view(-dist if way == 0 else dist, self.place.core, half)
            self._arrived(block, n, self.place.side(way))
            if (way, dist + 1, half) in self.keys:
                self.push((way, dist + 1, half))
            self._go(block, len(self.keys) + n, self.place.sibling())

    def arrive(self):
        for n, (way, dist, half) in enumerate(self.keys):
            block = self.view(-dist if way == 0 else dist, 1 - self.place.core, half)
            self._arrived(block, len(self.keys) + n, self.place.sibling())
        block = self.buf.at[self.place.column(0, 1 - self.place.core)]
        self._arrived(block, 2 * len(self.keys), self.place.sibling())

    def close(self):
        for copy in self.started:
            copy.wait_send()


def layer_kernel(
    ep_count, tp_count, seq_len,
    moe_in, moe_gain, routes, scores, shared_gate, shared_up, shared_down, mix_w_in, mix_w_out,
    mix_in, mix_gain, pool_mat, pool_scale, exp_gate, exp_up, exp_down,
    mixed, moe_out,
    tokens, outgoing, received, results, returned, pick, share, total, w_in, w_out,
    gate_w, up_w, down_w, gate_sum, up_sum, from_sibling, sums, arrived, tail, prior,
    ws, xs, xr, ins, inr, outs, outr, as_, ar, bs, br, hs, hr, ss, sr, rs, rr,
):
    place = Place(ep_count, tp_count)
    devices = ep_count * tp_count
    flat = place.ep * tp_count + place.tp
    after, before = (flat + 1) % devices, (flat + devices - 1) % devices
    after = (after // tp_count, after % tp_count)
    before = (before // tp_count, before % tp_count)
    loads = [
        pltpu.make_async_copy(src.at[0], dst, ws.at[n])
        for n, (src, dst) in enumerate(((exp_gate, gate_w), (exp_up, up_w), (exp_down, down_w)))
    ]
    for load in loads:
        load.start()
    greet([place.side(0), place.side(1), place.sibling(), after, before] + place.peers())
    me = place.tp
    rows, width = moe_in.shape
    pieces, cut = tokens.shape[0], tokens.shape[3]
    capacity = outgoing.shape[2]
    slots = ep_count * capacity
    block_rows = tp_count * rows
    far = place.far
    sent = []

    normed = rms_rows(moe_in[...], moe_gain[...])
    for c in range(pieces):
        tokens[c, pl.ds(me, 1)] = normed[:, c * cut : (c + 1) * cut][None]
    gathers = [RingGather(place, tokens.at[c], xs.at[c], xr.at[c]) for c in range(pieces)]
    gathers[0].start()
    gathers[1].start()

    top_count = routes.shape[0]
    lines = max(8, ep_count)
    names = lax.broadcasted_iota(jnp.int32, (lines, block_rows), 0) * tp_count + me
    score_sum = jnp.sum(scores[...], axis=0, keepdims=True)
    named = jnp.zeros((lines, block_rows), jnp.float32)
    weight = jnp.zeros((lines, block_rows), jnp.float32)
    for k in range(top_count):
        hit = routes[k : k + 1, :] == names
        named = named + jnp.where(hit, 1.0, 0.0)
        weight = weight + jnp.where(hit, scores[k : k + 1, :] / score_sum * ROUTED_SCALE, 0.0)
    ones = named.astype(jnp.bfloat16)
    earlier = []
    for low in range(0, block_rows, 512):
        source = lax.broadcasted_iota(jnp.int32, (block_rows, 512), 0)
        target = lax.broadcasted_iota(jnp.int32, (block_rows, 512), 1) + low
        strict = jnp.where(source < target, 1.0, 0.0).astype(jnp.bfloat16)
        earlier.append(jnp.dot(ones, strict, preferred_element_type=jnp.float32))
    spot = jnp.where(named > 0.5, jnp.concatenate(earlier, axis=1), -1.0).astype(jnp.int32)
    slot = lax.broadcasted_iota(jnp.int32, (capacity, block_rows), 0)
    for j in range(ep_count):
        here = spot[j : j + 1, :] == slot
        span = slice(j * capacity, (j + 1) * capacity)
        pick[span, :] = jnp.where(here, 1.0, 0.0).astype(jnp.bfloat16)
        weighed = jnp.where(here, weight[j : j + 1, :], 0.0).T.astype(jnp.bfloat16)
        share[:, :, span] = weighed.reshape(tp_count, rows, capacity)

    def scatter(source, landing, c, send, recv):
        for i, (peer, column) in enumerate(place.peers()):
            copy = remote(
                source.at[c, peer], landing.at[c, place.ep], send.at[c, i], recv.at[c, i],
                (peer, column),
            )
            copy.start()
            sent.append(copy)
        landing[c, pl.ds(place.ep, 1)] = source[c, pl.ds(place.ep, 1)]

    def landing_wait(landing, c, send, recv):
        for i in range(1, ep_count):
            peer = (place.ep - i + ep_count) % ep_count
            block = landing.at[c, peer]
            remote(block, block, send.at[c, i - 1], recv.at[c, i - 1], (peer, me)).wait_recv()

    for c in range(pieces):
        for dist in range(1, far + 1):
            gathers[c].step(dist)
            if dist == 1 and c + 2 < pieces:
                gathers[c + 2].start()
        gathers[c].arrive()
        picked = jnp.dot(
            pick[...], tokens[c].reshape(block_rows, cut), preferred_element_type=jnp.float32
        )
        outgoing[c] = picked.astype(jnp.bfloat16).reshape(ep_count, capacity, cut)
        scatter(outgoing, received, c, as_, ar)

    w_in[pl.ds(me, 1)] = mix_w_in[...][None]
    w_out[pl.ds(me, 1)] = mix_w_out[...][None]
    first = RingGather(place, w_in, ins, inr)
    second = RingGather(place, w_out, outs, outr)
    first.start()
    second.start()

    def ffn(i, carry):
        across = (((1,), (1,)), ((), ()))
        pair = pl.ds(i * CORES, CORES)
        gate = jnp.zeros((CORES * rows, shared_gate.shape[0]), jnp.float32)
        up = gate
        for c in range(pieces):
            block = tokens[c, pair].reshape(CORES * rows, cut)
            span = slice(c * cut, (c + 1) * cut)
            gate = gate + lax.dot_general(
                block, shared_gate[:, span], across, preferred_element_type=jnp.float32
            )
            up = up + lax.dot_general(
                block, shared_up[:, span], across, preferred_element_type=jnp.float32
            )
        hidden = (jax.nn.silu(gate) * up).astype(jnp.bfloat16)
        for c in range(pieces):
            value = jnp.dot(
                hidden, shared_down[:, c * cut : (c + 1) * cut], preferred_element_type=jnp.float32
            )
            total[c, pair] = value.astype(jnp.bfloat16).reshape(CORES, rows, cut)
        return carry

    lax.fori_loop(0, tp_count // CORES, ffn, 0)

    for load in loads:
        load.wait()
    for c in range(pieces):
        landing_wait(received, c, as_, ar)
        block = received[c].reshape(slots, cut)
        for acc, weights in ((gate_sum, gate_w), (up_sum, up_w)):
            value = jnp.dot(
                block, weights[c * cut : (c + 1) * cut, :], preferred_element_type=jnp.float32
            )
            acc[...] = value if c == 0 else acc[...] + value
    hidden = (jax.nn.silu(gate_sum[...]) * up_sum[...]).astype(jnp.bfloat16)
    for c in range(pieces):
        value = jnp.dot(
            hidden, down_w[:, c * cut : (c + 1) * cut], preferred_element_type=jnp.float32
        )
        results[c] = value.astype(jnp.bfloat16).reshape(ep_count, capacity, cut)
        scatter(results, returned, c, bs, br)

    for dist in range(1, far + 1):
        first.step(dist)
        second.step(dist)

    order = [far]
    for dist in range(far - 1, 0, -1):
        order += [dist, -dist]
    order += [0]
    half_rows = rows // 2
    keys = ring_keys(place.chips)

    def halves(half):
        return pl.ds(half * half_rows, half_rows)

    def landed(c, key):
        n = keys.index(key)
        block = arrived.at[c, n]
        remote(block, block, rs.at[c, n], rr.at[c, n], place.side(key[0])).wait_recv()
        return arrived[c, n].astype(jnp.float32)

    def chip_sum(c, chip, half):
        mine = total[c, pl.ds(chip * CORES + place.core, 1), halves(half)]
        theirs = from_sibling[c, pl.ds(chip, 1), halves(half)]
        return (mine.astype(jnp.float32) + theirs.astype(jnp.float32))[0]

    def sibling_wait(c, n):
        block = from_sibling.at[c, place.at(order[n])]
        remote(block, block, ss.at[c, n], sr.at[c, n], place.sibling()).wait_recv()

    def pass_on(c, n):
        step = order[n]
        dist = abs(step)
        sibling_wait(c, n)
        ways = (0, 1) if dist == far else ((0,) if step > 0 else (1,))
        for k, (way, d, half) in enumerate(keys):
            if d != dist or way not in ways:
                continue
            value = chip_sum(c, place.at(step), half)
            if (way, dist + 1, half) in keys:
                value = value + landed(c, (way, dist + 1, half))
            sums[c, k] = value.astype(jnp.bfloat16)
            copy = remote(
                sums.at[c, k], arrived.at[c, k], rs.at[c, k], rr.at[c, k], place.side(way)
            )
            copy.start()
            sent.append(copy)

    for c in range(pieces):
        landing_wait(returned, c, bs, br)
        for n, step in enumerate(order):
            chip = place.at(step)
            pair = pl.ds(chip * CORES, CORES)
            value = jnp.dot(
                share[pair].reshape(CORES * rows, slots),
                returned[c].reshape(slots, cut),
                preferred_element_type=jnp.float32,
            ).reshape(CORES, rows, cut)
            total[c, pair] = (value + total[c, pair].astype(jnp.float32)).astype(jnp.bfloat16)
            copy = remote(
                total.at[c, chip * CORES + 1 - place.core], from_sibling.at[c, chip],
                ss.at[c, n], sr.at[c, n], place.sibling(),
            )
            copy.start()
            sent.append(copy)
        pass_on(c, 0)

    first.arrive()
    second.arrive()
    groups, group_ch = pool_mat.shape[0], pool_mat.shape[1]
    reach = 2**groups
    mix_normed = rms_rows(mix_in[...], mix_gain[...])
    projected = jnp.dot(
        mix_normed, w_in[...].reshape(width, groups * group_ch), preferred_element_type=jnp.float32
    ).astype(jnp.bfloat16)
    tail[...] = projected[rows - reach :]
    halo = remote(tail, prior, hs, hr, after)
    halo.start()
    for n in range(1, len(order) - 1):
        for c in range(pieces):
            pass_on(c, n)
    halo.wait()
    first_row = flat * rows
    keep = jnp.where(first_row % seq_len == 0, 0.0, 1.0)
    extended = jnp.concatenate(
        [prior[...].astype(jnp.float32) * keep, projected.astype(jnp.float32)], axis=0
    )
    position = (first_row + lax.broadcasted_iota(jnp.int32, (rows, group_ch), 0)) % seq_len
    pooled_parts = []
    for group in range(groups):
        channels = slice(group * group_ch, (group + 1) * group_ch)
        running = extended[:, channels]
        for level in range(group + 1):
            running = running + pltpu.roll(running, 2**level, 0)
        counts = jnp.minimum(position + 1, 2 ** (group + 1)).astype(jnp.float32)
        pooled = (running[reach:] / counts - extended[reach:, channels]).astype(jnp.bfloat16)
        grouped = jnp.dot(pooled, pool_mat[group], preferred_element_type=jnp.float32)
        pooled_parts.append((grouped * pool_scale[:, channels]).astype(jnp.bfloat16))
    pool_out = jnp.concatenate(pooled_parts, axis=1)
    span = w_out.shape[2]
    for column in range(tp_count):
        mixed[:, column * span : (column + 1) * span] = jnp.dot(
            pool_out, w_out[column], preferred_element_type=jnp.float32
        ).astype(jnp.bfloat16)

    for c in range(pieces):
        sibling_wait(c, len(order) - 1)
        for half in range(2):
            value = chip_sum(c, place.chip, half)
            for way in range(2):
                if (way, 1, half) in keys:
                    value = value + landed(c, (way, 1, half))
            moe_out[half * half_rows : (half + 1) * half_rows, c * cut : (c + 1) * cut] = (
                value.astype(jnp.bfloat16)
            )
    for copy in sent:
        copy.wait_send()
    for gather in gathers + [first, second]:
        gather.close()


def vmem(count):
    return [pl.BlockSpec(memory_space=pltpu.VMEM)] * count


def shards(
    mix_in, mix_gain, mix_w_in, pool_mat, pool_scale, mix_w_out, moe_in, moe_gain, routes,
    route_score, exp_gate, exp_up, exp_down, shared_gate, shared_up, shared_down,
):
    ep_count, tp_count = lax.axis_size("ep"), lax.axis_size("tp")
    rows, width = moe_in.shape
    block_rows, top_count = routes.shape
    capacity = 2 * block_rows * top_count // (ep_count * tp_count)
    slots = ep_count * capacity
    dma = lambda n: pltpu.SemaphoreType.DMA((n,))
    bf16 = jnp.bfloat16
    messages = len(ring_keys(tp_count // CORES))

    chips = tp_count // CORES
    pieces = 4
    cut = width // pieces
    hidden = exp_gate.shape[2]
    reach = 2 ** pool_mat.shape[0]
    seq_len = mix_in.shape[0] * ep_count * tp_count // SEQS_MIX
    grid = lambda n: pltpu.SemaphoreType.DMA((pieces, n))
    buffer = lambda *shape: pltpu.VMEM(shape, bf16)
    mixed, moe_out = pl.pallas_call(
        functools.partial(layer_kernel, ep_count, tp_count, seq_len),
        out_shape=[
            jax.ShapeDtypeStruct(mix_in.shape, bf16),
            jax.ShapeDtypeStruct(moe_in.shape, bf16),
        ],
        in_specs=vmem(13) + [pl.BlockSpec(memory_space=pl.ANY)] * 3,
        out_specs=vmem(2),
        scratch_shapes=[
            buffer(pieces, tp_count, rows, cut),
            buffer(pieces, ep_count, capacity, cut),
            buffer(pieces, ep_count, capacity, cut),
            buffer(pieces, ep_count, capacity, cut),
            buffer(pieces, ep_count, capacity, cut),
            buffer(slots, block_rows),
            buffer(tp_count, rows, slots),
            buffer(pieces, tp_count, rows, cut),
            buffer(tp_count, *mix_w_in.shape),
            buffer(tp_count, *mix_w_out.shape),
            buffer(width, hidden),
            buffer(width, hidden),
            buffer(hidden, width),
            pltpu.VMEM((slots, hidden), jnp.float32),
            pltpu.VMEM((slots, hidden), jnp.float32),
            buffer(pieces, chips, rows, cut),
            buffer(pieces, messages, rows // 2, cut),
            buffer(pieces, messages, rows // 2, cut),
            buffer(reach, mix_w_in.shape[1]),
            buffer(reach, mix_w_in.shape[1]),
            dma(3),
            grid(2 * messages + 1),
            grid(2 * messages + 1),
        ]
        + [dma(2 * messages + 1) for _ in range(4)]
        + [grid(ep_count - 1) for _ in range(4)]
        + [pltpu.SemaphoreType.DMA, pltpu.SemaphoreType.DMA]
        + [grid(chips), grid(chips), grid(messages), grid(messages)],
        compiler_params=pltpu.CompilerParams(
            collective_id=0, has_side_effects=True, vmem_limit_bytes=67043328
        ),
    )(
        moe_in, moe_gain[None, :], routes.T, route_score.T.astype(jnp.float32), shared_gate,
        shared_up, shared_down, mix_w_in, mix_w_out, mix_in, mix_gain[None, :], pool_mat,
        pool_scale[None, :], exp_gate, exp_up, exp_down,
    )
    return (mixed, moe_out)


def solution(mesh):
    return jax.shard_map(
        shards,
        mesh=mesh,
        in_specs=(
            P(("ep", "tp"), None),
            P(),
            P("tp", None),
            P(),
            P(),
            P(None, "tp"),
            P(("ep", "tp"), None),
            P(),
            P("ep", None),
            P("ep", None),
            P(("ep", "tp"), None, None),
            P(("ep", "tp"), None, None),
            P(("ep", "tp"), None, None),
            P("tp", None),
            P("tp", None),
            P("tp", None),
        ),
        out_specs=(P(("ep", "tp"), None), P(("ep", "tp"), None)),
        check_vma=False,
    )
```

time: 215 us -> 132 us (0.61)
  Pallas kernels: 166 us -> 126 us
  local copies, waits for them, and re-layouts: 20.8 us -> 3.76 us
  matrix products: 13.8 us -> 0 us
  other arithmetic: 12.9 us -> 1.29 us
    pallas_call x2 -> x1, Pallas kernels: 166 us -> 126 us  [shards(): pl.pallas_call(functools.partial(layer_kernel, ep_count, tp_count, seq_le...]
    dot_general x2 -> x0, matrix products: 13.8 us -> none  [the longest x1 8.33 us: shards(): jnp.dot(hidden, exp_down[0], preferred_element_type=jnp.float32)]
    eq x3 -> x0, local copies, waits for them, and re-layouts: 7.98 us -> none  [the longest x2 7.98 us: shards(): spot[:, :, None] == slot[None, None, :]]
    broadcast_in_dim x2 -> x0, local copies, waits for them, and re-layouts: 4.33 us -> none  [shards(): jnp.where(spot[:, :, None] == slot[None, None, :], weight[:, :, None], 0.0)]
    another operation x2 -> x0, other arithmetic: 3.64 us -> none
    convert_element_type x2 -> x1, other arithmetic: 4.63 us -> 1.29 us  [shards(): route_score.T.astype(jnp.float32)]
    concatenate x1 -> x0, other arithmetic: 2.2 us -> none  [shards(): jnp.concatenate([jnp.pad(shared_gate, pad), jnp.pad(shared_up, pad)], axi...]
    unnamed x25 -> x2, local copies, waits for them, and re-layouts: 5.58 us -> 3.76 us
where the time goes in v2:
time: 132 us; the launch traced here: 131 us
  Pallas kernels  126 us (95%)
  local copies, waits for them, and re-layouts  3.76 us (3%)
    pallas_call x1, Pallas kernels, shards(): pl.pallas_call(functools.partial(layer_kernel, ep_count, tp_count, seq_le...  126 us
    unnamed x2, local copies, waits for them, and re-layouts  3.76 us

profile of v2, /device:TPU:0, one launch (start us, length us, event | category | flops | bytes accessed | tf_op | source)
XLA Modules:
  0.0 131.5 jit_solution(12201692519339006460)
XLA Ops:
  0.6 1.3 convert_bitcast_fusion.scores
  1.9 125.8 %shard_map.167 = (bf16[128,2048]{1,0:T(8,128)(2,1)}, bf16[128,2048]{1,0:T(8,128)(2,1)}) custom-call(bf16[128,2048]{1,0:T(8,128)(2,1)} %moe_in.1, f32[1,2048]{1,0:T(1,128)} %bitcast.6, s32[2,1024]{1,0:T(2,128)} %bitcast.7, f32[2,1024]{1,0:T(2,128)} %convert_bitcast_fusion.scores, bf16[96,2048]{1,0:T(8,128)(2,1)} %shared_gate.1, bf16[96,2048]{1,0:T(8,128)(2,1)} %shared_up.1, ...), custom_call_target="tpu_custom_call" | custom-call | tf_op jit(solution)/shard_map/pallas_call | solution.py:417
  127.7 1.9 %copy.20 = bf16[128,2048]{1,0:T(8,128)(2,1)} copy(bf16[128,2048]{1,0:T(8,128)(2,1)} %get-tuple-element.4) | data formatting | bytes 1048576
  129.6 1.9 %copy.21 = bf16[128,2048]{1,0:T(8,128)(2,1)} copy(bf16[128,2048]{1,0:T(8,128)(2,1)} %get-tuple-element.5) | data formatting | bytes 1048576
